TPU v7x, 32 devices: a whole 2x2x4 slice. The times are simulated.
32 devices in a mesh: ep: 16 (over z, x, core), tp: 2 (over y).
Axes of the slice: x: 2, y: 2, z: 4, core: 2. Of those that a mesh axis runs over, the one named last changes fastest.
Arguments:
- tokens: bfloat16 [208, 1024], P('ep'), may hold values from -60 to 60
- attn_gain: float32 [1024], replicated, may hold values from 0.1 to 1.9
- query_weight: bfloat16 [1024, 512], P(None, 'tp'), may hold values from -0.1875 to 0.1875
- key_weight: bfloat16 [1024, 256], P(None, 'tp'), may hold values from -0.1875 to 0.1875
- value_weight: bfloat16 [1024, 256], P(None, 'tp'), may hold values from -0.1875 to 0.1875
- forget_weight: bfloat16 [1024, 8], P(None, 'tp'), may hold values from -0.5 to 0.5
- forget_bias: float32 [8], P('tp'), may hold values from -3 to 3
- out_weight: bfloat16 [512, 1024], P('tp'), may hold values from -0.75 to 0.75
- key_cache: bfloat16 [208, 4, 64, 1024], P('ep', 'tp'), may hold values from -300 to 300
- value_cache: bfloat16 [208, 4, 64, 1024], P('ep', 'tp'), may hold values from -12 to 12
- cum_forget: float32 [208, 8, 1024], P('ep', 'tp'), may hold values from -131 to 0, as said below
- lengths: int32 [208], P('ep'), may hold values from 256 to 1024
- ffn_gain: float32 [1024], replicated, may hold values from 0.1 to 1.9
- routes: int32 [208, 2], P('ep'), may hold values from 0 to 3, all different within a row; in each aligned block of 13 rows (0 to 12, 13 to 25, ...) at most 13 rows name the same one
- route_weights: float32 [208, 2], P('ep'), may hold values from 0.2 to 1
- gate_weight: bfloat16 [16, 1024, 512], P('ep', None, 'tp'), may hold values from -0.1875 to 0.1875
- up_weight: bfloat16 [16, 1024, 512], P('ep', None, 'tp'), may hold values from -0.1875 to 0.1875
- down_weight: bfloat16 [16, 512, 1024], P('ep', 'tp'), may hold values from -0.25 to 0.25
Outputs:
- layer_out: bfloat16 [208, 1024], P('ep', 'tp')
Inputs may be any that keep to these rules, and one draw needn't show every extreme that they name: `routes`: the experts of a row differ; in each aligned block of 13 rows (the rows of one index of ep) no expert is named by more than 13 rows. `cum_forget`: for each sequence and head the entries do not increase along positions.
All inputs are finite; a program needn't handle non-finite values.
Results may differ from a plain program's by a relative error of at most 0.0085.
Values may be sent and summed in bfloat16 or wider, within the bound.
A program may use at most 64 MiB of HBM per device.

v0:
```python
import jax
import jax.numpy as jnp
from jax import lax
from jax.sharding import PartitionSpec as P

HEADS = 8
KVH = 4
HD = 64
SLICES = 4
TOP_K = 2
STORED_SPAN = 1024


EPSILON = 1e-06


def round_trip(values):
    return lax.optimization_barrier(values.astype(jnp.bfloat16)).astype(jnp.float32)


def inverse_rms(values, width):
    return lax.rsqrt(jnp.sum(values * values, axis=-1, keepdims=True) / width + EPSILON)


def body(
    tokens,
    attn_gain,
    query_weight,
    key_weight,
    value_weight,
    forget_weight,
    forget_bias,
    out_weight,
    key_cache,
    value_cache,
    cum_forget,
    lengths,
    ffn_gain,
    routes,
    route_weights,
    gate_weight,
    up_weight,
    down_weight,
):
    tp_count = lax.axis_size("tp")
    ep_count = lax.axis_size("ep")
    tp_rank = lax.axis_index("tp")
    seq_rows = tokens.shape[0]
    width = tokens.shape[1]
    cols = width // tp_count
    experts = ep_count // SLICES
    capacity = min(seq_rows, max(2, (2 * seq_rows * TOP_K + experts - 1) // experts))
    kv_local = key_cache.shape[1]
    group = HEADS // KVH
    score_scale = HD ** (-0.5)
    token_f = tokens.astype(jnp.float32)
    normed = (token_f * inverse_rms(token_f, width) * attn_gain).astype(jnp.bfloat16)
    query_rows = jnp.dot(normed, query_weight, preferred_element_type=jnp.float32).astype(
        jnp.bfloat16
    )
    query_rows = query_rows.reshape(seq_rows, kv_local, group, HD)
    fresh_keys = jnp.dot(normed, key_weight, preferred_element_type=jnp.float32).astype(
        jnp.bfloat16
    )
    fresh_keys = fresh_keys.reshape(seq_rows, kv_local, HD)
    new_values = jnp.dot(normed, value_weight, preferred_element_type=jnp.float32).astype(
        jnp.bfloat16
    )
    new_values = new_values.reshape(seq_rows, kv_local, HD)
    log_forget = jax.nn.log_sigmoid(
        jnp.dot(normed, forget_weight, preferred_element_type=jnp.float32) + forget_bias
    )
    log_forget = log_forget.reshape(seq_rows, kv_local, group)
    scores = (
        jnp.einsum("bkgd,bkdl->bkgl", query_rows, key_cache, preferred_element_type=jnp.float32)
        * score_scale
    )
    cumul = cum_forget.reshape(seq_rows, kv_local, group, STORED_SPAN)
    last_index = jnp.broadcast_to(
        (lengths - 1)[:, None, None, None], (seq_rows, kv_local, group, 1)
    )
    last = jnp.take_along_axis(cumul, last_index, axis=3)
    positions = lax.broadcasted_iota(jnp.int32, (1, 1, 1, STORED_SPAN), 3)
    valid = positions < lengths[:, None, None, None]
    scores = jnp.where(valid, scores + (last - cumul) + log_forget[..., None], -jnp.inf)
    self_score = (
        jnp.einsum("qvml,qvl->qvm", query_rows, fresh_keys, preferred_element_type=jnp.float32)
        * score_scale
    )
    top = jnp.maximum(jnp.max(scores, axis=3), self_score)
    expo = jnp.exp(scores - top[..., None])
    own_exp = jnp.exp(self_score - top)
    total = jnp.sum(expo, axis=3) + own_exp
    attn_weights = (expo / total[..., None]).astype(jnp.bfloat16)
    own_weight = round_trip(own_exp / total)
    heads_out = jnp.einsum(
        "bkgl,bkdl->bkgd", attn_weights, value_cache, preferred_element_type=jnp.float32
    )
    heads_out = heads_out + own_weight[..., None] * new_values.astype(jnp.float32)[:, :, None, :]
    heads_out = heads_out.astype(jnp.bfloat16).reshape(seq_rows, -1)
    partial_value = jnp.dot(heads_out, out_weight, preferred_element_type=jnp.float32)
    mixed = lax.psum(partial_value.astype(jnp.bfloat16), "tp").astype(jnp.float32)
    residual = round_trip(token_f + mixed)
    sent = (residual * inverse_rms(residual, width) * ffn_gain).astype(jnp.bfloat16)
    residual_cols = lax.dynamic_slice_in_dim(residual, tp_rank * cols, cols, 1)
    assigned = routes.reshape(-1)
    member = (assigned[:, None] == lax.broadcasted_iota(jnp.int32, (1, experts), 1)).astype(
        jnp.int32
    )
    earlier = jnp.cumsum(member, axis=0) - member
    slots = assigned * capacity + jnp.sum(earlier * member, axis=1)
    place = (slots[None, :] == lax.broadcasted_iota(jnp.int32, (experts * capacity, 1), 0)).astype(
        jnp.bfloat16
    )
    spread_rows = jnp.repeat(sent, TOP_K, axis=0)
    outgoing = jnp.dot(place, spread_rows, preferred_element_type=jnp.float32).astype(jnp.bfloat16)
    row_width = outgoing.shape[1]
    outgoing = jnp.broadcast_to(
        outgoing.reshape(experts, 1, capacity, row_width), (experts, SLICES, capacity, row_width)
    ).reshape(ep_count, capacity, row_width)
    gate_local = gate_weight[0]
    up_local = up_weight[0]
    down_local = down_weight[0]
    arrived = lax.all_to_all(outgoing, "ep", split_axis=0, concat_axis=0, tiled=True)
    slot_count = arrived.shape[1]
    flat = arrived.reshape(-1, width)
    gate = jnp.dot(flat, gate_local, preferred_element_type=jnp.float32)
    up = jnp.dot(flat, up_local, preferred_element_type=jnp.float32)
    hidden = (jax.nn.silu(gate) * up).astype(jnp.bfloat16)
    part = jnp.dot(hidden, down_local, preferred_element_type=jnp.float32)
    part = part.reshape(arrived.shape[0], slot_count, width)
    summed = lax.psum_scatter(part.astype(jnp.bfloat16), "tp", scatter_dimension=2, tiled=True)
    returned = lax.all_to_all(summed, "ep", split_axis=0, concat_axis=0, tiled=True)
    per_slot = jnp.sum(
        returned.astype(jnp.float32).reshape(experts, SLICES, capacity, cols), axis=1
    )
    per_slot = per_slot.reshape(experts * capacity, cols)
    picked = jnp.take(per_slot, slots, axis=0).reshape(seq_rows, TOP_K, cols)
    routed = jnp.sum(route_weights[:, :, None] * picked, axis=1)
    return (residual_cols + routed).astype(jnp.bfloat16)


def solution(mesh):
    return jax.shard_map(
        body,
        mesh=mesh,
        in_specs=(
            P("ep", None),
            P(),
            P(None, "tp"),
            P(None, "tp"),
            P(None, "tp"),
            P(None, "tp"),
            P("tp"),
            P("tp", None),
            P("ep", "tp", None, None),
            P("ep", "tp", None, None),
            P("ep", "tp", None),
            P("ep"),
            P(),
            P("ep", None),
            P("ep", None),
            P("ep", None, "tp"),
            P("ep", None, "tp"),
            P("ep", "tp", None),
        ),
        out_specs=P("ep", "tp"),
        check_vma=False,
    )
```

profile of v0, /device:TPU:0, one launch (start us, length us, event | category | flops | bytes accessed | tf_op | source)
XLA Modules:
  0.0 109.5 jit_solution(850440614468388697)
XLA Ops:
  6.5 0.8 broadcast_add_fusion
  7.3 0.8 broadcast_compare_fusion
  8.2 0.7 iota_compare_fusion
  9.2 1.8 %reshape.179 = f32[13,2,2,1024]{3,2,1,0:T(2,128)} reshape(f32[13,4,1024]{2,1,0:T(4,128)} %param.28) | data formatting | bytes 425984 | tf_op jit(solution)/shard_map/reshape | solution.py:78
  11.0 2.4 %gather_fusion.1 = f32[52]{0:T(128)S(1)} fusion(f32[13,2,2,1024]{3,2,1,0:T(2,128)} %reshape.179, s32[52]{0:T(128)S(1)} %reshape.202), kind=kCustom, calls=%fused_computation.1 | custom fusion | bytes 1248 | tf_op jit(solution)/shard_map/jit(take_along_axis)/gather | solution.py:82
  13.8 1.3 %convolution_convert_fusion.3 = bf16[13,256]{1,0:T(8,128)(2,1)S(1)} fusion(bf16[1024,256]{1,0:T(8,128)(2,1)} %param.20, bf16[13,1024]{1,0:T(8,128)(2,1)S(1)} %copy-done.1, f32[1024]{0:T(1024)S(1)} %copy-done.6, f32[13]{0:T(128)S(1)} %add_rsqrt_fusion.1), kind=kOutput, calls=%fused_computation.13 | convolution fusion | flops 6872320 | bytes 561716 | tf_op jit(solution)/shard_map/dot_general | solution.py:58
  15.5 1.2 %convolution_convert_fusion.5 = bf16[13,128]{1,0:T(8,128)(2,1)S(1)} fusion(bf16[1024,128]{1,0:T(8,128)(2,1)} %param.21, bf16[13,1024]{1,0:T(8,128)(2,1)S(1)} %copy-done.1, f32[1024]{0:T(1024)S(1)} %copy-done.6, f32[13]{0:T(128)S(1)} %add_rsqrt_fusion.1), kind=kOutput, calls=%fused_computation.16 | convolution fusion | flops 3462784 | bytes 296244 | tf_op jit(solution)/shard_map/dot_general | solution.py:62
  17.0 1.6 %fusion.35 = (f32[13,2,2]{2,1,0:T(2,128)S(1)}, f32[13,2,2,1024]{3,2,1,0:T(2,128)S(1)}) fusion(f32[13,2,2]{2,1,0:T(2,128)S(1)} %copy.40, f32[13,2,2,1024]{3,2,1,0:T(2,128)} %reshape.179, f32[13,2,2]{2,1,0:T(2,128)S(1)} %and_select_fusion, bf16[13,2,2,64]{3,2,1,0:T(2,128)(2,1)S(1)} %reshape.178, bf16[13,2,64,1024]{3,2,1,0:T(8,128)(2,1)S(1)} %copy-done, ...), kind=kOutput, calls=%fused_computation.81 | convolution fusion | flops 7135180 | bytes 3854448 | tf_op jit(solution)/shard_map/bkgd,bkdl->bkgl/dot_general | solution.py:75
  18.6 0.7 copy-done.2
  19.9 3.2 %fusion.4 = bf16[13,2,2,64]{3,2,1,0:T(2,128)(2,1)S(1)} fusion(bf16[13,2,64,1024]{3,2,1,0:T(8,128)(2,1)} %param.27, f32[13,2,2,1024]{3,2,1,0:T(2,128)} %copy-done.2, f32[13,2,2]{2,1,0:T(2,128)S(1)} %get-tuple-element.6, f32[13,2,2]{2,1,0:T(2,128)S(1)} %multiply_maximum_fusion, f32[13,2,64]{2,1,0:T(2,128)S(1)} %reshape.189, ...), kind=kOutput, calls=%fused_computation.12 | convolution fusion | flops 6985472 | bytes 3634800 | tf_op jit(solution)/shard_map/bkgl,bkdl->bkgd/dot_general | solution.py:96
  23.2 1.2 %convolution_convert_fusion.2 = bf16[13,1024]{1,0:T(8,128)(2,1)S(1)} fusion(bf16[13,256]{1,0:T(8,128)(2,1)S(1)} %reshape.181, bf16[256,1024]{1,0:T(8,128)(2,1)} %param.25), kind=kOutput, calls=%fused_computation.10 | convolution fusion | flops 6829056 | bytes 557568 | tf_op jit(solution)/shard_map/dot_general | solution.py:101
  24.4 10.0 %psum.7 = bf16[13,1024]{1,0:T(8,128)(2,1)S(1)} all-reduce(bf16[13,1024]{1,0:T(8,128)(2,1)S(1)} %convolution_convert_fusion.2), channel_id=1, replica_groups=mesh['ep'=16,'tp'=2] {'tp'}, use_global_device_ids=true, to_apply=%region_3.4 | all-reduce | flops 13312 | bytes 53248 | tf_op jit(solution)/shard_map/psum | solution.py:102
  34.6 0.6 reshape.183
  36.3 1.0 convolution_convert_fusion.1
  37.3 0.7 broadcast_in_dim.75
  38.0 1.0 broadcast_in_dim.76
  39.0 20.0 %all_to_all.10 = bf16[16,13,1024]{2,1,0:T(8,128)(2,1)} all-to-all(bf16[16,13,1024]{2,1,0:T(8,128)(2,1)S(1)} %bitcast.42), channel_id=1, replica_groups=mesh['ep'=16,'tp'=2] {'ep'}, dimensions={0} | all-to-all | bytes 851968 | tf_op jit(solution)/shard_map/all_to_all | solution.py:124
  58.9 2.0 %reshape.185 = bf16[208,1024]{1,0:T(8,128)(2,1)} reshape(bf16[16,13,1024]{2,1,0:T(8,128)(2,1)} %all_to_all.10) | data formatting | bytes 851968 | tf_op jit(solution)/shard_map/reshape | solution.py:126
  60.9 1.4 %fusion.9 = f32[208,256]{1,0:T(8,128)S(1)} fusion(bf16[208,1024]{1,0:T(8,128)(2,1)} %reshape.185, bf16[1,1024,256]{2,1,0:T(8,128)(2,1)} %param.33), kind=kOutput, calls=%fused_computation.22 | convolution fusion | flops 109051904 | bytes 1163264 | tf_op jit(solution)/shard_map/dot_general | solution.py:127
  62.3 1.5 %fusion.3 = bf16[208,256]{1,0:T(8,128)(2,1)S(1)} fusion(bf16[208,1024]{1,0:T(8,128)(2,1)} %reshape.185, bf16[1,1024,256]{2,1,0:T(8,128)(2,1)} %param.34, f32[208,256]{1,0:T(8,128)S(1)} %fusion.9), kind=kOutput, calls=%fused_computation.9 | convolution fusion | flops 109371392 | bytes 1269760 | tf_op jit(solution)/shard_map/dot_general | solution.py:128
  63.8 0.7 dot_general.49
  64.5 2.2 %convolution_convert_fusion = bf16[16,13,1024]{2,0,1:T(8,128)(2,1)} fusion(bf16[1,256,1024]{2,1,0:T(8,128)(2,1)} %param.35, bf16[16,13,256]{2,1,0:T(8,128)(2,1)} %dot_general.49), kind=kOutput, calls=%fused_computation.2 | convolution fusion | flops 109264896 | bytes 1056768 | tf_op jit(solution)/shard_map/dot_general | solution.py:130
  66.9 12.1 %reduce-scatter.2.cloned.1.call-done = bf16[16,13,512]{2,0,1:T(8,128)(2,1)} async-done(((bf16[16,13,1024]{2,0,1:T(8,128)(2,1)}), bf16[16,13,512]{2,0,1:T(8,128)(2,1)}) %reduce-scatter.2.cloned.1.call-update) | async-done | bytes 213008 | tf_op jit(solution)/shard_map/reduce_scatter | solution.py:132
  78.9 1.8 %copy.46 = bf16[16,13,512]{2,1,0:T(8,128)(2,1)} copy(bf16[16,13,512]{2,0,1:T(8,128)(2,1)} %reduce-scatter.2.cloned.1.call-done) | data formatting | bytes 425984 | tf_op jit(solution)/shard_map/reduce_scatter | solution.py:132
  80.7 5.7 %all-to-all-start.1 = ((bf16[16,13,512]{2,1,0:T(8,128)(2,1)}), bf16[16,13,512]{2,1,0:T(8,128)(2,1)}, u32[]{:S(2)}, u32[]{:S(2)}) async-start(bf16[16,13,512]{2,1,0:T(8,128)(2,1)} %copy.46), calls=%async_computation.2 | async-start | bytes 524288 | tf_op jit(solution)/shard_map/all_to_all | solution.py:133
  87.3 0.8 copy.41
  88.1 8.4 %all-to-all-done.1 = bf16[16,13,512]{2,1,0:T(8,128)(2,1)} async-done(((bf16[16,13,512]{2,1,0:T(8,128)(2,1)}), bf16[16,13,512]{2,1,0:T(8,128)(2,1)}, u32[]{:S(2)}, u32[]{:S(2)}) %all-to-all-start.1) | async-done | bytes 213024 | tf_op jit(solution)/shard_map/all_to_all | solution.py:133
  96.4 1.7 %convert_reduce_fusion = f32[4,13,512]{2,1,0:T(8,128)} fusion(bf16[16,13,512]{2,1,0:T(8,128)(2,1)} %all-to-all-done.1), kind=kLoop, calls=%fused_computation.19 | loop fusion | flops 186368 | bytes 319488 | tf_op jit(solution)/shard_map/reduce_sum | solution.py:134
  98.1 0.9 reshape.188
  99.0 1.2 %gather_fusion = f32[26,512]{1,0:T(8,128)} fusion(f32[52,512]{1,0:T(8,128)S(1)} %reshape.188, s32[1024]{0:T(1024)S(1)} %pad_clamp_fusion), kind=kCustom, calls=%fused_computation | custom fusion | bytes 106600 | tf_op jit(solution)/shard_map/jit(_take)/gather | solution.py:138
  100.2 0.9 gather.15
  101.3 1.4 %add_convert_fusion = bf16[13,512]{1,0:T(8,128)(2,1)} fusion(f32[13,512]{1,0:T(8,128)S(1)} %multiply_reduce_fusion.1, f32[13,1024]{1,0:T(8,128)} %convert_element_type.83, s32[]{:T(128)S(6)} %select_n.74), kind=kLoop, calls=%fused_computation.41 | loop fusion | flops 13312 | bytes 66564 | tf_op jit(solution)/shard_map/convert_element_type | solution.py:140
  (72 shorter events, 4.6 us)
Async XLA Ops:
  6.5 10.4 %copy-start = (bf16[13,2,64,1024]{3,2,1,0:T(8,128)(2,1)S(1)}, bf16[13,2,64,1024]{3,2,1,0:T(8,128)(2,1)}, u32[]{:S(2)}) copy-start(bf16[13,2,64,1024]{3,2,1,0:T(8,128)(2,1)} %param.26) | copy-start | bytes 10223620
  6.5 72.4 %reduce-scatter.2.cloned.1.call-start = ((), (), s32[]{:S(2)}) async-start(), calls=%async_computation.3 | async-start | bytes 638976 | tf_op jit(solution)/shard_map/reduce_scatter | solution.py:132
  11.0 2.7 %copy-start.1 = (bf16[13,1024]{1,0:T(8,128)(2,1)S(1)}, bf16[13,1024]{1,0:T(8,128)(2,1)}, u32[]{:S(2)}) copy-start(bf16[13,1024]{1,0:T(8,128)(2,1)} %param.18) | copy-start | bytes 79876
  11.0 2.8 %copy-start.6 = (f32[1024]{0:T(1024)S(1)}, f32[1024]{0:T(1024)}, u32[]{:S(2)}) copy-start(f32[1024]{0:T(1024)} %param.19) | copy-start | bytes 12292
  11.0 4.2 %copy-start.10 = (bf16[1024,4]{0,1:T(4,128)(2,1)S(1)}, bf16[1024,4]{0,1:T(4,128)(2,1)}, u32[]{:S(2)}) copy-start(bf16[1024,4]{0,1:T(4,128)(2,1)} %param.23) | copy-start | bytes 24580
  11.0 4.2 %copy-start.11 = (f32[4]{0:T(128)S(1)}, f32[4]{0:T(128)}, u32[]{:S(2)}) copy-start(f32[4]{0:T(128)} %param.24) | copy-start | bytes 52
  16.8 2.8 %copy-start.9 = (bf16[1024,128]{1,0:T(8,128)(2,1)S(1)}, bf16[1024,128]{1,0:T(8,128)(2,1)}, u32[]{:S(2)}) copy-start(bf16[1024,128]{1,0:T(8,128)(2,1)} %param.22) | copy-start | bytes 786436
  18.6 0.7 copy-start.2
  19.8 14.7 %copy-start.5 = (f32[1024]{0:T(1024)S(1)}, f32[1024]{0:T(1024)}, u32[]{:S(2)}) copy-start(f32[1024]{0:T(1024)} %param.30) | copy-start | bytes 12292
  19.9 15.4 %copy-start.3 = (s32[13,2]{0,1:T(2,128)S(1)}, s32[13,2]{0,1:T(2,128)}, u32[]{:S(2)}) copy-start(s32[13,2]{0,1:T(2,128)} %param.31) | copy-start | bytes 316
  35.8 0.5 copy-start.7
  38.9 27.7 %copy-start.8 = (s32[26]{0:T(128)S(1)}, s32[26]{0:T(128)}, u32[]{:S(2)}) copy-start(s32[26]{0:T(128)} %copy-done.7) | copy-start | bytes 316
  38.9 27.9 %copy-start.4 = (s32[13,2]{0,1:T(2,128)S(1)}, s32[13,2]{0,1:T(2,128)}, u32[]{:S(2)}) copy-start(s32[13,2]{0,1:T(2,128)} %param.31) | copy-start | bytes 316
  80.7 15.7 %all-to-all-start.1 = ((bf16[16,13,512]{2,1,0:T(8,128)(2,1)}), bf16[16,13,512]{2,1,0:T(8,128)(2,1)}, u32[]{:S(2)}, u32[]{:S(2)}) async-start(bf16[16,13,512]{2,1,0:T(8,128)(2,1)} %copy.46), calls=%async_computation.2 | async-start | bytes 524288 | tf_op jit(solution)/shard_map/all_to_all | solution.py:133
Sparse Core Ops, SparseCore 0:
  66.8 12.1 reduce-scatter.1
where the time goes:
time: 110 us; the launch traced here: 109 us
  blocking collectives  29.9 us (27%)
  waiting for transfers between devices  20.5 us (19%)
  local copies, waits for them, and re-layouts  17.4 us (16%)
  matrix products  15 us (14%)
  between operations  13.7 us (12%)
  other arithmetic  7.39 us (7%)
  starting transfers between devices  5.67 us (5%)
    all_to_all x1, blocking collectives, body(): lax.all_to_all(outgoing, 'ep', split_axis=0, concat_axis=0, tiled=True)  20 us
    reduce_scatter x1, waiting for transfers between devices, body(): lax.psum_scatter(part.astype(jnp.bfloat16), 'tp', scatter_dimension=2, ti...  12.1 us
    psum x1, blocking collectives, body(): lax.psum(partial_value.astype(jnp.bfloat16), 'tp').astype(jnp.float32)  9.95 us
    all_to_all x1, waiting for transfers between devices, body(): lax.all_to_all(summed, 'ep', split_axis=0, concat_axis=0, tiled=True)  8.35 us
    all_to_all x1, starting transfers between devices, body(): lax.all_to_all(summed, 'ep', split_axis=0, concat_axis=0, tiled=True)  5.67 us
    dot_general x1, matrix products, body(): jnp.einsum('bkgl,bkdl->bkgd', attn_weights, value_cache, preferred_elemen...  3.15 us
    gather x5, local copies, waits for them, and re-layouts, body(): last = jnp.take_along_axis(cumul, last_index, axis=3)  2.75 us
  transfers between devices with their start and end apart: 2, of which 2 were waited for; matrix products, arithmetic and copies ran while one was open for 2% of the time, Pallas kernels for 0%

commit v1 on v0

v1 whole, which is shorter than its diff:
```python
import functools

import jax
import jax.numpy as jnp
from jax import lax
from jax.experimental import pallas as pl
from jax.experimental.pallas import tpu as pltpu
from jax.sharding import PartitionSpec as P

HEADS = 8
KVH = 4
HD = 64
SLICES = 4
EPSILON = 1e-06
GROUP_SEQS = 4
MESH = pl.DeviceIdType.MESH
F32 = jnp.float32
BF16 = jnp.bfloat16


def inverse_rms(values):
    return lax.rsqrt(jnp.sum(values * values, axis=-1, keepdims=True) / values.shape[-1] + EPSILON)


def dot(a, b):
    return jnp.dot(a, b, preferred_element_type=F32)


def dot_nt(a, b):
    return lax.dot_general(a, b, (((1,), (1,)), ((), ())), preferred_element_type=F32)


def attention_kernel(
    tokens_ref,
    gain_ref,
    bias_ref,
    lengths_ref,
    wq_hbm,
    wk_hbm,
    wv_hbm,
    wf_ref,
    wo_hbm,
    keys_hbm,
    values_hbm,
    cum_hbm,
    part_ref,
    wq,
    wk,
    wv,
    wo,
    keys,
    values,
    cum,
    q_rows,
    own_rows,
    out_rows,
    w_sem,
    k_sem,
    v_sem,
    c_sem,
):
    rows = tokens_ref.shape[0]
    kv_local, hd, span = keys.shape[1:]
    heads = cum.shape[1]
    group = heads // kv_local
    lanes = kv_local * hd
    scale = hd ** (-0.5)
    w_copies = [
        pltpu.make_async_copy(src, dst, w_sem.at[i])
        for i, (src, dst) in enumerate(((wq_hbm, wq), (wk_hbm, wk), (wv_hbm, wv), (wo_hbm, wo)))
    ]
    for copy in w_copies[:3]:
        copy.start()
    copies = []
    for b in range(rows):
        trio = (
            pltpu.make_async_copy(keys_hbm.at[b], keys.at[b], k_sem.at[b]),
            pltpu.make_async_copy(cum_hbm.at[b], cum.at[b], c_sem.at[b]),
            pltpu.make_async_copy(values_hbm.at[b], values.at[b], v_sem.at[b]),
        )
        for copy in trio:
            copy.start()
        copies.append(trio)
    w_copies[3].start()

    token_f = tokens_ref[...].astype(F32)
    normed = (token_f * inverse_rms(token_f) * gain_ref[...]).astype(BF16)
    head_id = lax.broadcasted_iota(jnp.int32, (heads, 1), 0)
    bias = jnp.zeros((heads, 1), F32)
    for h in range(heads):
        bias = jnp.where(head_id == h, bias_ref[h], bias)
    log_forget = jax.nn.log_sigmoid(dot_nt(wf_ref[...], normed) + bias)
    for copy in w_copies[:3]:
        copy.wait()
    queries = dot(normed, wq[...]).astype(BF16).astype(F32)
    new_keys = dot(normed, wk[...]).astype(BF16).astype(F32)
    new_values = dot(normed, wv[...]).astype(BF16).astype(F32)
    lane_kv = lax.broadcasted_iota(jnp.int32, (rows, lanes), 1) // hd
    q_rows[...] = jnp.zeros_like(q_rows)
    own_rows[...] = jnp.zeros_like(own_rows)
    for h in range(heads):
        kv = h // group
        base = (h * hd) // lanes * lanes
        segment = queries[:, base : base + lanes]
        shift = (kv * hd - (h * hd - base)) % lanes
        if shift:
            segment = pltpu.roll(segment, shift, 1)
        segment = jnp.where(lane_kv == kv, segment, 0.0)
        q_rows[pl.ds(h, rows, stride=8), :] = segment
        own_rows[pl.ds(h, rows, stride=8), :] = segment * new_keys

    position = lax.broadcasted_iota(jnp.int32, (heads, span), 1)
    for first in range(0, rows, GROUP_SEQS):
        members = range(first, min(first + GROUP_SEQS, rows))
        for b in members:
            for copy in copies[b]:
                copy.wait()
        scores = [
            dot(q_rows[b * 8 : b * 8 + 8, :].astype(BF16), keys[b].reshape(lanes, span))[:heads]
            for b in members
        ]
        weights, own = [], []
        for b, score in zip(members, scores):
            cumul = cum[b]
            length = lengths_ref[b]
            last = jnp.sum(jnp.where(position == length - 1, cumul, 0.0), axis=1, keepdims=True)
            score = score * scale + (last - cumul) + log_forget[:, b : b + 1]
            score = jnp.where(position < length, score, -jnp.inf)
            self_score = (
                jnp.sum(own_rows[b * 8 : b * 8 + 8, :], axis=1, keepdims=True)[:heads] * scale
            )
            top = jnp.maximum(jnp.max(score, axis=1, keepdims=True), self_score)
            expo = jnp.exp(score - top)
            own_exp = jnp.exp(self_score - top)
            inverse = 1.0 / (jnp.sum(expo, axis=1, keepdims=True) + own_exp)
            weights.append((expo * inverse).astype(BF16))
            own.append((own_exp * inverse).astype(BF16).astype(F32))
        for b, weight, own_weight in zip(members, weights, own):
            mixed = dot_nt(weight, values[b].reshape(lanes, span))
            out_rows[b * 8 : b * 8 + heads, :] = mixed + own_weight * new_values[b : b + 1, :]

    blocks = []
    for h in range(heads):
        kv = h // group
        base = (h * hd) // lanes * lanes
        segment = out_rows[pl.ds(h, rows, stride=8), :]
        segment = jnp.where(lane_kv == kv, segment, 0.0)
        shift = (h * hd - base - kv * hd) % lanes
        if shift:
            segment = pltpu.roll(segment, shift, 1)
        if base // lanes == len(blocks):
            blocks.append(segment)
        else:
            blocks[-1] = blocks[-1] + segment
    w_copies[3].wait()
    total = None
    for i, block in enumerate(blocks):
        term = dot(block.astype(BF16), wo[i * lanes : (i + 1) * lanes, :])
        total = term if total is None else total + term
    part_ref[...] = jnp.zeros_like(part_ref)
    part_ref[0:rows, :] = total.astype(BF16)


def experts_kernel(
    outer,
    part_ref,
    tokens_ref,
    gain_ref,
    routes_ref,
    route_weights_ref,
    gate_hbm,
    up_hbm,
    down_hbm,
    out_ref,
    gate,
    up,
    down,
    part_in,
    residual,
    xbuf,
    core_out,
    core_in,
    core_own,
    plane,
    plane_in,
    back_out,
    back_in,
    w_sem,
    t_sem,
    z_send,
    a_send,
    c_send,
    x_recv,
    core_sem,
    plane_send,
    plane_recv,
    back_send,
    back_recv,
):
    rows, width = tokens_ref.shape
    pad = part_ref.shape[0]
    cols = out_ref.shape[1]
    me, t = lax.axis_index("ep"), lax.axis_index("tp")
    o, a, c = me // SLICES, (me // 2) % 2, me % 2
    na, nc, nt = 1 - a, 1 - c, 1 - t

    def device(o_, a_, c_, t_):
        return (o_ * SLICES + a_ * 2 + c_, t_)

    def send(src, dst, s_sem, r_sem, target):
        copy = pltpu.make_async_remote_copy(
            src_ref=src,
            dst_ref=dst,
            send_sem=s_sem,
            recv_sem=r_sem,
            device_id=target,
            device_id_type=MESH,
        )
        copy.start()
        sent.append(copy)
        return copy

    sent = []
    w_copies = [
        pltpu.make_async_copy(src.at[0], dst, w_sem.at[i])
        for i, (src, dst) in enumerate(((gate_hbm, gate), (up_hbm, up), (down_hbm, down)))
    ]
    barrier = pltpu.get_barrier_semaphore()
    others = [lax.rem(o + i, outer) for i in range(1, outer)]
    peers = [device(o_, a, c, t) for o_ in others]
    peers += [device(o, na, c, t), device(o, a, nc, t), device(o, a, c, nt), device(o, na, c, nt)]
    for peer in peers:
        pl.semaphore_signal(barrier, inc=1, device_id=peer, device_id_type=MESH)
    for copy in w_copies:
        copy.start()
    pl.semaphore_wait(barrier, len(peers))

    swap = send(part_ref, part_in, t_sem.at[0], t_sem.at[1], device(o, a, c, nt))
    swap.wait_recv()
    token_f = tokens_ref[...].astype(F32)
    mixed = part_ref[0:rows, :].astype(F32) + part_in[0:rows, :].astype(F32)
    mixed = mixed.astype(BF16).astype(F32)
    summed = (token_f + mixed).astype(BF16).astype(F32)
    for i in range(width // cols):
        residual[i, 0:rows, :] = summed[:, i * cols : (i + 1) * cols]
    ffn_in = (summed * inverse_rms(summed) * gain_ref[...]).astype(BF16)
    xbuf[c, a, o] = jnp.zeros((pad, width), BF16)
    xbuf[c, a, o, 0:rows, :] = ffn_in

    mine = xbuf.at[c, a, o]
    for i, o_ in enumerate(others):
        send(mine, mine, z_send.at[i], x_recv.at[c, a, o], device(o_, a, c, t))
    order = [o] + others
    for i, o_ in enumerate(order):
        block, sem = xbuf.at[c, a, o_], x_recv.at[c, a, o_]
        if i:
            pltpu.make_async_copy(block, block, sem).wait()
        send(block, block, a_send.at[i], sem, device(o, na, c, t))
        send(block, block, c_send.at[0, i], sem, device(o, a, nc, t))
    for i, o_ in enumerate(order):
        block, sem = xbuf.at[c, na, o_], x_recv.at[c, na, o_]
        pltpu.make_async_copy(block, block, sem).wait()
        send(block, block, c_send.at[1, i], sem, device(o, a, nc, t))
    for copy in w_copies:
        copy.wait()

    def experts(half):
        x = half.reshape(2 * outer * pad, width)
        g = dot(x, gate[...])
        hidden = (g / (1.0 + jnp.exp(-g)) * dot(x, up[...])).astype(BF16)
        return dot(hidden, down[...]).reshape(2, outer, pad, width)

    for a_ in (a, na):
        for o_ in order:
            block, sem = xbuf.at[nc, a_, o_], x_recv.at[nc, a_, o_]
            pltpu.make_async_copy(block, block, sem).wait()
    core_out[...] = experts(xbuf[nc]).astype(BF16)
    swap = send(core_out, core_in, core_sem.at[0], core_sem.at[1], device(o, a, nc, t))
    core_own[...] = experts(xbuf[c])
    swap.wait_recv()
    for i in range(width // cols):
        at = slice(i * cols, (i + 1) * cols)
        plane[:, i] = (core_own[:, :, :, at] + core_in[:, :, :, at].astype(F32)).astype(BF16)
    hops = [
        send(
            plane.at[a_, t_],
            plane_in.at[i],
            plane_send.at[i],
            plane_recv.at[i],
            device(o, a_, c, t_),
        )
        for i, (a_, t_) in enumerate(((na, nt), (na, t), (a, nt)))
    ]
    total = plane[a, t].astype(F32)
    for i in (1, 2, 0):
        hops[i].wait_recv()
        total = total + plane_in[i].astype(F32)
    back_out[...] = total.astype(BF16)
    for i, o_ in enumerate(others):
        send(
            back_out.at[o_], back_in.at[o], back_send.at[i], back_recv.at[o], device(o_, a, c, t)
        )
    back_in[o] = back_out[o]
    for o_ in others:
        block = back_in.at[o_]
        pltpu.make_async_copy(block, block, back_recv.at[o_]).wait()
    result = residual[t, 0:rows, :]
    routes = routes_ref[...]
    route_weights = route_weights_ref[...]
    for e in range(outer):
        weight = jnp.sum(jnp.where(routes == e, route_weights, 0.0), axis=1, keepdims=True)
        result = result + weight * back_in[e, 0:rows, :].astype(F32)
    out_ref[...] = result.astype(BF16)
    for copy in sent:
        copy.wait_send()


def body(
    tokens,
    attn_gain,
    query_weight,
    key_weight,
    value_weight,
    forget_weight,
    forget_bias,
    out_weight,
    key_cache,
    value_cache,
    cum_forget,
    lengths,
    ffn_gain,
    routes,
    route_weights,
    gate_weight,
    up_weight,
    down_weight,
):
    tp_count = lax.axis_size("tp")
    outer = lax.axis_size("ep") // SLICES
    rows, width = tokens.shape
    cols = width // tp_count
    pad = (rows + 15) // 16 * 16
    kv_local, hd, span = key_cache.shape[1:]
    heads = cum_forget.shape[1]
    lanes = kv_local * hd
    units = gate_weight.shape[2]
    hbm, vmem, smem = (
        pl.BlockSpec(memory_space=space) for space in (pltpu.HBM, pltpu.VMEM, pltpu.SMEM)
    )
    dma = pltpu.SemaphoreType.DMA
    part = pl.pallas_call(
        attention_kernel,
        out_shape=jax.ShapeDtypeStruct((pad, width), BF16),
        in_specs=[vmem, vmem, smem, smem, hbm, hbm, hbm, vmem, hbm, hbm, hbm, hbm],
        out_specs=vmem,
        scratch_shapes=[
            pltpu.VMEM(query_weight.shape, BF16),
            pltpu.VMEM(key_weight.shape, BF16),
            pltpu.VMEM(value_weight.shape, BF16),
            pltpu.VMEM(out_weight.shape, BF16),
            pltpu.VMEM(key_cache.shape, BF16),
            pltpu.VMEM(value_cache.shape, BF16),
            pltpu.VMEM(cum_forget.shape, F32),
            pltpu.VMEM((pad * 8, lanes), F32),
            pltpu.VMEM((pad * 8, lanes), F32),
            pltpu.VMEM((pad * 8, lanes), F32),
            dma((4,)),
            dma((rows,)),
            dma((rows,)),
            dma((rows,)),
        ],
        compiler_params=pltpu.CompilerParams(vmem_limit_bytes=24 * 2**20),
        name="attention",
    )(
        tokens,
        attn_gain.reshape(1, width),
        forget_bias,
        lengths,
        query_weight,
        key_weight,
        value_weight,
        forget_weight.T,
        out_weight,
        key_cache,
        value_cache,
        cum_forget,
    )
    return pl.pallas_call(
        functools.partial(experts_kernel, outer),
        out_shape=jax.ShapeDtypeStruct((rows, cols), BF16),
        in_specs=[vmem] * 5 + [hbm] * 3,
        out_specs=vmem,
        scratch_shapes=[
            pltpu.VMEM(gate_weight.shape[1:], BF16),
            pltpu.VMEM(up_weight.shape[1:], BF16),
            pltpu.VMEM(down_weight.shape[1:], BF16),
            pltpu.VMEM((pad, width), BF16),
            pltpu.VMEM((tp_count, pad, cols), F32),
            pltpu.VMEM((2, 2, outer, pad, width), BF16),
            pltpu.VMEM((2, outer, pad, width), BF16),
            pltpu.VMEM((2, outer, pad, width), BF16),
            pltpu.VMEM((2, outer, pad, width), F32),
            pltpu.VMEM((2, tp_count, outer, pad, cols), BF16),
            pltpu.VMEM((3, outer, pad, cols), BF16),
            pltpu.VMEM((outer, pad, cols), BF16),
            pltpu.VMEM((outer, pad, cols), BF16),
            dma((3,)),
            dma((2,)),
            dma((outer - 1,)),
            dma((outer,)),
            dma((2, outer)),
            dma((2, 2, outer)),
            dma((2,)),
            dma((3,)),
            dma((3,)),
            dma((outer - 1,)),
            dma((outer,)),
        ],
        compiler_params=pltpu.CompilerParams(
            collective_id=0, has_side_effects=True, vmem_limit_bytes=48 * 2**20
        ),
        name="experts",
    )(
        part,
        tokens,
        ffn_gain.reshape(1, width),
        routes,
        route_weights,
        gate_weight,
        up_weight,
        down_weight,
    )


def solution(mesh):
    return jax.shard_map(
        body,
        mesh=mesh,
        in_specs=(
            P("ep", None),
            P(),
            P(None, "tp"),
            P(None, "tp"),
            P(None, "tp"),
            P(None, "tp"),
            P("tp"),
            P("tp", None),
            P("ep", "tp", None, None),
            P("ep", "tp", None, None),
            P("ep", "tp", None),
            P("ep"),
            P(),
            P("ep", None),
            P("ep", None),
            P("ep", None, "tp"),
            P("ep", None, "tp"),
            P("ep", "tp", None),
        ),
        out_specs=P("ep", "tp"),
        check_vma=False,
    )
```

time: 110 us -> 48.7 us (0.44)
  Pallas kernels: 0 us -> 33.6 us
  blocking collectives: 29.9 us -> 0 us
  waiting for transfers between devices: 20.5 us -> 0 us
  matrix products: 15 us -> 0 us
  between operations: 13.7 us -> 0.08 us
  other arithmetic: 7.39 us -> 0 us
  starting transfers between devices: 5.67 us -> 0 us
  local copies, waits for them, and re-layouts: 17.4 us -> 14.5 us
    pallas_call x0 -> x2, Pallas kernels: none -> 33.6 us  [the longest x1 27.9 us: body(): pl.pallas_call(functools.partial(experts_kernel, outer), out_shape=jax.Sh...]
    all_to_all x1 -> x0, blocking collectives: 20 us -> none  [body(): lax.all_to_all(outgoing, 'ep', split_axis=0, concat_axis=0, tiled=True)]
    dot_general x12 -> x0, matrix products: 15 us -> none  [the longest x1 3.15 us: body(): jnp.einsum('bkgl,bkdl->bkgd', attn_weights, value_cache, preferred_elemen...]
    unnamed x29 -> x37, local copies, waits for them, and re-layouts: 2.09 us -> 14.5 us
    reduce_scatter x1 -> x0, waiting for transfers between devices: 12.1 us -> none  [body(): lax.psum_scatter(part.astype(jnp.bfloat16), 'tp', scatter_dimension=2, ti...]
    psum x1 -> x0, blocking collectives: 9.95 us -> none  [body(): lax.psum(partial_value.astype(jnp.bfloat16), 'tp').astype(jnp.float32)]
    all_to_all x1 -> x0, waiting for transfers between devices: 8.35 us -> none  [body(): lax.all_to_all(summed, 'ep', split_axis=0, concat_axis=0, tiled=True)]
    reshape x8 -> x0, local copies, waits for them, and re-layouts: 5.68 us -> none  [the longest x1 1.95 us: body(): flat = arrived.reshape(-1, width)]
  transfers between devices with their start and end apart: 2 -> 0, of which waited for: 2 -> 0; matrix products, arithmetic and copies ran while one was open for 2% -> 0% of each run, Pallas kernels for 0% -> 0%
where the time goes in v1:
time: 48.7 us; the launch traced here: 48.1 us
  Pallas kernels  33.6 us (69%)
  local copies, waits for them, and re-layouts  14.5 us (30%)
    pallas_call x1, Pallas kernels, body(): pl.pallas_call(functools.partial(experts_kernel, outer), out_shape=jax.Sh...  27.9 us
    unnamed x37, local copies, waits for them, and re-layouts  14.5 us
    pallas_call x1, Pallas kernels, body(): pl.pallas_call(attention_kernel, out_shape=jax.ShapeDtypeStruct((pad, wid...  5.68 us

profile of v1, /device:TPU:0, one launch (start us, length us, event | category | flops | bytes accessed | tf_op | source)
XLA Modules:
  0.0 48.1 jit_solution(8869439885714482048)
XLA Ops:
  0.0 0.8 %copy.19.routes_ref = s32[13,2]{1,0:T(8,128)S(1)} copy(s32[13,2]{0,1:T(2,128)} %param.31) | data formatting | bytes 208 | tf_op args[13]
  0.8 0.8 %copy.20.route_weights_ref = f32[13,2]{1,0:T(8,128)S(1)} copy(f32[13,2]{0,1:T(2,128)} %param.32) | data formatting | bytes 208 | tf_op args[14]
  1.5 0.0 copy-start
  1.5 2.0 %copy-done = bf16[13,2,64,1024]{3,2,1,0:T(8,128)(2,1)S(1)} copy-done((bf16[13,2,64,1024]{3,2,1,0:T(8,128)(2,1)S(1)}, bf16[13,2,64,1024]{3,2,1,0:T(8,128)(2,1)}, u32[]{:S(2)}) %copy-start) | copy-done | bytes 3407896
  3.5 0.0 copy-start.1
  3.5 2.0 %copy-done.1 = bf16[13,2,64,1024]{3,2,1,0:T(8,128)(2,1)S(1)} copy-done((bf16[13,2,64,1024]{3,2,1,0:T(8,128)(2,1)S(1)}, bf16[13,2,64,1024]{3,2,1,0:T(8,128)(2,1)}, u32[]{:S(2)}) %copy-start.1) | copy-done | bytes 3407896
  5.5 0.0 copy-start.2
  5.5 1.0 %copy-done.2 = bf16[1024,256]{1,0:T(8,128)(2,1)S(1)} copy-done((bf16[1024,256]{1,0:T(8,128)(2,1)S(1)}, bf16[1024,256]{1,0:T(8,128)(2,1)}, u32[]{:S(2)}) %copy-start.2) | copy-done | bytes 524312
  6.5 0.0 copy-start.3
  6.5 1.0 %copy-done.3 = bf16[256,1024]{1,0:T(8,128)(2,1)S(1)} copy-done((bf16[256,1024]{1,0:T(8,128)(2,1)S(1)}, bf16[256,1024]{1,0:T(8,128)(2,1)}, u32[]{:S(2)}) %copy-start.3) | copy-done | bytes 524312
  7.5 0.0 copy-start.7
  7.5 0.9 %copy-done.7 = bf16[1024,128]{1,0:T(8,128)(2,1)S(1)} copy-done((bf16[1024,128]{1,0:T(8,128)(2,1)S(1)}, bf16[1024,128]{1,0:T(8,128)(2,1)}, u32[]{:S(2)}) %copy-start.7) | copy-done | bytes 262168
  8.5 0.9 %copy-done.8 = bf16[1024,128]{1,0:T(8,128)(2,1)S(1)} copy-done((bf16[1024,128]{1,0:T(8,128)(2,1)S(1)}, bf16[1024,128]{1,0:T(8,128)(2,1)}, u32[]{:S(2)}) %copy-start.8) | copy-done | bytes 262168
  9.4 0.0 copy-start.9
  9.4 0.9 %copy-done.9 = f32[13,4,1024]{2,1,0:T(4,128)S(1)} copy-done((f32[13,4,1024]{2,1,0:T(4,128)S(1)}, f32[13,4,1024]{2,1,0:T(4,128)}, u32[]{:S(2)}) %copy-start.9) | copy-done | bytes 213016
  10.4 0.0 copy-start.10
  10.4 0.8 %copy-done.10 = bf16[13,1024]{1,0:T(8,128)(2,1)S(1)} copy-done((bf16[13,1024]{1,0:T(8,128)(2,1)S(1)}, bf16[13,1024]{1,0:T(8,128)(2,1)}, u32[]{:S(2)}) %copy-start.10) | copy-done | bytes 26648
  11.1 0.0 copy-start.12
  11.1 0.7 %copy-done.12 = bf16[1024,4]{0,1:T(4,128)(2,1)S(1)} copy-done((bf16[1024,4]{0,1:T(4,128)(2,1)S(1)}, bf16[1024,4]{0,1:T(4,128)(2,1)}, u32[]{:S(2)}) %copy-start.12) | copy-done | bytes 8216
  11.8 0.0 copy-start.13
  11.8 0.7 %copy-done.13 = f32[1024]{0:T(1024)S(1)} copy-done((f32[1024]{0:T(1024)S(1)}, f32[1024]{0:T(1024)}, u32[]{:S(2)}) %copy-start.13) | copy-done | bytes 4120
  12.5 0.7 %copy-done.15 = f32[4]{0:T(128)S(1)} copy-done((f32[4]{0:T(128)S(1)}, f32[4]{0:T(128)}, u32[]{:S(2)}) %copy-start.15) | copy-done | bytes 40
  13.2 0.7 %copy-done.16 = s32[13]{0:T(128)S(1)} copy-done((s32[13]{0:T(128)S(1)}, s32[13]{0:T(128)}, u32[]{:S(2)}) %copy-start.16) | copy-done | bytes 76
  13.8 0.0 copy-start.14
  13.9 5.7 %attention.1.part_ref = bf16[16,1024]{1,0:T(8,128)(2,1)S(1)} custom-call(bf16[13,1024]{1,0:T(8,128)(2,1)S(1)} %copy-done.10, f32[1,1024]{1,0:T(1,128)S(1)} %bitcast.4, f32[4]{0:T(128)S(1)} %copy-done.15, s32[13]{0:T(128)S(1)} %copy-done.16, bf16[1024,256]{1,0:T(8,128)(2,1)S(1)} %copy-done.2, bf16[1024,128]{1,0:T(8,128)(2,1)S(1)} %copy-done.7, ...), custom_call_target="tpu_custom_call" | custom-call | tf_op jit(solution)/shard_map/attention/pallas_call | solution.py:351
  19.5 0.0 copy-done.4
  19.6 0.0 copy-done.5
  19.6 0.0 copy-done.6
  19.6 0.0 copy-done.11
  19.6 0.0 copy-done.14
  19.6 27.9 %experts.1 = bf16[13,512]{1,0:T(8,128)(2,1)S(1)} custom-call(bf16[16,1024]{1,0:T(8,128)(2,1)S(1)} %attention.1.part_ref, bf16[13,1024]{1,0:T(8,128)(2,1)S(1)} %copy-done.11, f32[1,1024]{1,0:T(1,128)S(1)} %bitcast.5, s32[13,2]{1,0:T(8,128)S(1)} %copy.19.routes_ref, f32[13,2]{1,0:T(8,128)S(1)} %copy.20.route_weights_ref, bf16[1,1024,256]{2,1,0:T(8,128)(2,1)S(1)} %copy-done.4, ...), custom_call_target="tpu_custom_call" | custom-call | tf_op jit(solution)/shard_map/experts/pallas_call | solution.py:388
  47.5 0.6 %copy.22 = bf16[13,512]{1,0:T(8,128)(2,1)} copy(bf16[13,512]{1,0:T(8,128)(2,1)S(1)} %experts.1) | data formatting | bytes 26624
  (7 shorter events, 0.0 us)
Async XLA Ops:
  1.5 2.0 %copy-start = (bf16[13,2,64,1024]{3,2,1,0:T(8,128)(2,1)S(1)}, bf16[13,2,64,1024]{3,2,1,0:T(8,128)(2,1)}, u32[]{:S(2)}) copy-start(bf16[13,2,64,1024]{3,2,1,0:T(8,128)(2,1)} %keys_hbm.1) | copy-start | bytes 10223620
  3.5 2.0 %copy-start.1 = (bf16[13,2,64,1024]{3,2,1,0:T(8,128)(2,1)S(1)}, bf16[13,2,64,1024]{3,2,1,0:T(8,128)(2,1)}, u32[]{:S(2)}) copy-start(bf16[13,2,64,1024]{3,2,1,0:T(8,128)(2,1)} %values_hbm.1) | copy-start | bytes 10223620
  5.5 1.0 %copy-start.2 = (bf16[1024,256]{1,0:T(8,128)(2,1)S(1)}, bf16[1024,256]{1,0:T(8,128)(2,1)}, u32[]{:S(2)}) copy-start(bf16[1024,256]{1,0:T(8,128)(2,1)} %wq_hbm.1) | copy-start | bytes 1572868
  6.5 1.0 %copy-start.3 = (bf16[256,1024]{1,0:T(8,128)(2,1)S(1)}, bf16[256,1024]{1,0:T(8,128)(2,1)}, u32[]{:S(2)}) copy-start(bf16[256,1024]{1,0:T(8,128)(2,1)} %wo_hbm.1) | copy-start | bytes 1572868
  7.5 0.9 %copy-start.7 = (bf16[1024,128]{1,0:T(8,128)(2,1)S(1)}, bf16[1024,128]{1,0:T(8,128)(2,1)}, u32[]{:S(2)}) copy-start(bf16[1024,128]{1,0:T(8,128)(2,1)} %wk_hbm.1) | copy-start | bytes 786436
  8.5 0.9 %copy-start.8 = (bf16[1024,128]{1,0:T(8,128)(2,1)S(1)}, bf16[1024,128]{1,0:T(8,128)(2,1)}, u32[]{:S(2)}) copy-start(bf16[1024,128]{1,0:T(8,128)(2,1)} %wv_hbm.1) | copy-start | bytes 786436
  9.4 0.9 %copy-start.9 = (f32[13,4,1024]{2,1,0:T(4,128)S(1)}, f32[13,4,1024]{2,1,0:T(4,128)}, u32[]{:S(2)}) copy-start(f32[13,4,1024]{2,1,0:T(4,128)} %cum_hbm.1) | copy-start | bytes 638980
  10.4 0.8 %copy-start.10 = (bf16[13,1024]{1,0:T(8,128)(2,1)S(1)}, bf16[13,1024]{1,0:T(8,128)(2,1)}, u32[]{:S(2)}) copy-start(bf16[13,1024]{1,0:T(8,128)(2,1)} %tokens_ref.3) | copy-start | bytes 79876
  11.1 0.7 %copy-start.12 = (bf16[1024,4]{0,1:T(4,128)(2,1)S(1)}, bf16[1024,4]{0,1:T(4,128)(2,1)}, u32[]{:S(2)}) copy-start(bf16[1024,4]{0,1:T(4,128)(2,1)} %param.23) | copy-start | bytes 24580
  11.8 0.7 %copy-start.13 = (f32[1024]{0:T(1024)S(1)}, f32[1024]{0:T(1024)}, u32[]{:S(2)}) copy-start(f32[1024]{0:T(1024)} %param.19) | copy-start | bytes 12292
  12.5 0.7 %copy-start.15 = (f32[4]{0:T(128)S(1)}, f32[4]{0:T(128)}, u32[]{:S(2)}) copy-start(f32[4]{0:T(128)} %bias_ref.1) | copy-start | bytes 52
  13.2 0.7 %copy-start.16 = (s32[13]{0:T(128)S(1)}, s32[13]{0:T(128)}, u32[]{:S(2)}) copy-start(s32[13]{0:T(128)} %lengths_ref.1) | copy-start | bytes 160
  13.8 5.7 %copy-start.4 = (bf16[1,1024,256]{2,1,0:T(8,128)(2,1)S(1)}, bf16[1,1024,256]{2,1,0:T(8,128)(2,1)}, u32[]{:S(2)}) copy-start(bf16[1,1024,256]{2,1,0:T(8,128)(2,1)} %gate_hbm.1) | copy-start | bytes 1572868
  13.8 5.7 %copy-start.5 = (bf16[1,1024,256]{2,1,0:T(8,128)(2,1)S(1)}, bf16[1,1024,256]{2,1,0:T(8,128)(2,1)}, u32[]{:S(2)}) copy-start(bf16[1,1024,256]{2,1,0:T(8,128)(2,1)} %up_hbm.1) | copy-start | bytes 1572868
  13.8 5.7 %copy-start.6 = (bf16[1,256,1024]{2,1,0:T(8,128)(2,1)S(1)}, bf16[1,256,1024]{2,1,0:T(8,128)(2,1)}, u32[]{:S(2)}) copy-start(bf16[1,256,1024]{2,1,0:T(8,128)(2,1)} %down_hbm.1) | copy-start | bytes 1572868
  13.8 5.7 %copy-start.11 = (bf16[13,1024]{1,0:T(8,128)(2,1)S(1)}, bf16[13,1024]{1,0:T(8,128)(2,1)}, u32[]{:S(2)}) copy-start(bf16[13,1024]{1,0:T(8,128)(2,1)} %tokens_ref.3) | copy-start | bytes 79876
  13.8 5.7 %copy-start.14 = (f32[1024]{0:T(1024)S(1)}, f32[1024]{0:T(1024)}, u32[]{:S(2)}) copy-start(f32[1024]{0:T(1024)} %param.30) | copy-start | bytes 12292

commit v2 on v1

v2 whole, which is shorter than its diff:
```python
import functools

import jax
import jax.numpy as jnp
from jax import lax
from jax.experimental import pallas as pl
from jax.experimental.pallas import tpu as pltpu
from jax.sharding import PartitionSpec as P

HEADS = 8
KVH = 4
HD = 64
SLICES = 4
EPSILON = 1e-06
GROUP_SEQS = 4
MESH = pl.DeviceIdType.MESH
F32 = jnp.float32
BF16 = jnp.bfloat16


def inverse_rms(values):
    return lax.rsqrt(jnp.sum(values * values, axis=-1, keepdims=True) / values.shape[-1] + EPSILON)


def dot(a, b):
    return jnp.dot(a, b, preferred_element_type=F32)


def dot_nt(a, b):
    return lax.dot_general(a, b, (((1,), (1,)), ((), ())), preferred_element_type=F32)


def layer_kernel(
    outer,
    tokens_hbm,
    attn_gain_hbm,
    bias_hbm,
    lengths_hbm,
    wq_hbm,
    wk_hbm,
    wv_hbm,
    wf_hbm,
    wo_hbm,
    keys_hbm,
    values_hbm,
    cum_hbm,
    ffn_gain_hbm,
    routes_hbm,
    route_weights_hbm,
    gate_hbm,
    up_hbm,
    down_hbm,
    out_ref,
    tokens_ref,
    attn_gain_ref,
    bias_ref,
    lengths_ref,
    wq,
    wk,
    wv,
    wf_ref,
    wo,
    keys,
    values,
    cum,
    ffn_gain_ref,
    routes_ref,
    route_weights_ref,
    gate,
    up,
    down,
    q_rows,
    own_rows,
    out_rows,
    part,
    part_in,
    residual,
    xbuf,
    core_out,
    core_in,
    core_own,
    plane,
    plane_in,
    back_out,
    back_in,
    w_sem,
    k_sem,
    v_sem,
    c_sem,
    t_sem,
    z_send,
    a_send,
    c_send,
    x_recv,
    core_send,
    core_recv,
    plane_send,
    plane_recv,
    back_send,
    back_recv,
):
    rows, width = tokens_ref.shape
    pad = part.shape[0]
    cols = out_ref.shape[1]
    kv_local, hd, span = keys.shape[1:]
    heads = cum.shape[1]
    group = heads // kv_local
    lanes = kv_local * hd
    scale = hd ** (-0.5)
    me, t = lax.axis_index("ep"), lax.axis_index("tp")
    o, a, c = me // SLICES, (me // 2) % 2, me % 2
    na, nc, nt = 1 - a, 1 - c, 1 - t

    def local(i, src, dst):
        copy = pltpu.make_async_copy(src, dst, w_sem.at[i])
        copy.start()
        return copy

    first_copies = [
        local(i, src, dst)
        for i, (src, dst) in enumerate(
            (
                (tokens_hbm, tokens_ref),
                (attn_gain_hbm, attn_gain_ref),
                (bias_hbm, bias_ref),
                (lengths_hbm, lengths_ref),
                (wf_hbm, wf_ref),
                (wq_hbm, wq),
                (wk_hbm, wk),
                (wv_hbm, wv),
            )
        )
    ]

    def device(o_, a_, c_, t_):
        return (o_ * SLICES + a_ * 2 + c_, t_)

    near = sorted(range(1, outer), key=lambda i: min(i, outer - i))
    others = [lax.rem(o + i, outer) for i in near]
    barrier = pltpu.get_barrier_semaphore()
    peers = [device(o_, a, c, t) for o_ in others]
    peers += [device(o, na, c, t), device(o, a, nc, t), device(o, a, c, nt), device(o, na, c, nt)]
    for peer in peers:
        pl.semaphore_signal(barrier, inc=1, device_id=peer, device_id_type=MESH)

    copies = []
    for b in range(rows):
        trio = (
            pltpu.make_async_copy(keys_hbm.at[b], keys.at[b], k_sem.at[b]),
            pltpu.make_async_copy(cum_hbm.at[b], cum.at[b], c_sem.at[b]),
            pltpu.make_async_copy(values_hbm.at[b], values.at[b], v_sem.at[b]),
        )
        for copy in trio:
            copy.start()
        copies.append(trio)
    wo_copy = local(8, wo_hbm, wo)
    late_copies = [
        local(i + 9, src, dst)
        for i, (src, dst) in enumerate(
            (
                (ffn_gain_hbm, ffn_gain_ref),
                (routes_hbm, routes_ref),
                (route_weights_hbm, route_weights_ref),
                (gate_hbm.at[0], gate),
                (up_hbm.at[0], up),
                (down_hbm.at[0], down),
            )
        )
    ]

    for copy in first_copies:
        copy.wait()
    token_f = tokens_ref[...].astype(F32)
    normed = (token_f * inverse_rms(token_f) * attn_gain_ref[...]).astype(BF16)
    head_id = lax.broadcasted_iota(jnp.int32, (heads, 1), 0)
    bias = jnp.zeros((heads, 1), F32)
    for h in range(heads):
        bias = jnp.where(head_id == h, bias_ref[h], bias)
    log_forget = jax.nn.log_sigmoid(dot_nt(wf_ref[...], normed) + bias)
    queries = dot(normed, wq[...]).astype(BF16).astype(F32)
    new_keys = dot(normed, wk[...]).astype(BF16).astype(F32)
    new_values = dot(normed, wv[...]).astype(BF16).astype(F32)
    lane_kv = lax.broadcasted_iota(jnp.int32, (rows, lanes), 1) // hd
    q_rows[...] = jnp.zeros_like(q_rows)
    own_rows[...] = jnp.zeros_like(own_rows)
    for h in range(heads):
        kv = h // group
        base = (h * hd) // lanes * lanes
        segment = queries[:, base : base + lanes]
        shift = (kv * hd - (h * hd - base)) % lanes
        if shift:
            segment = pltpu.roll(segment, shift, 1)
        segment = jnp.where(lane_kv == kv, segment, 0.0)
        q_rows[pl.ds(h, rows, stride=8), :] = segment
        own_rows[pl.ds(h, rows, stride=8), :] = segment * new_keys

    position = lax.broadcasted_iota(jnp.int32, (heads, span), 1)
    for first in range(0, rows, GROUP_SEQS):
        members = range(first, min(first + GROUP_SEQS, rows))
        for b in members:
            for copy in copies[b]:
                copy.wait()
        scores = [
            dot(q_rows[b * 8 : b * 8 + 8, :].astype(BF16), keys[b].reshape(lanes, span))[:heads]
            for b in members
        ]
        weights, own = [], []
        for b, score in zip(members, scores):
            cumul = cum[b]
            length = lengths_ref[b]
            last = jnp.sum(jnp.where(position == length - 1, cumul, 0.0), axis=1, keepdims=True)
            score = score * scale + (last - cumul) + log_forget[:, b : b + 1]
            score = jnp.where(position < length, score, -jnp.inf)
            self_score = (
                jnp.sum(own_rows[b * 8 : b * 8 + 8, :], axis=1, keepdims=True)[:heads] * scale
            )
            top = jnp.maximum(jnp.max(score, axis=1, keepdims=True), self_score)
            expo = jnp.exp(score - top)
            own_exp = jnp.exp(self_score - top)
            inverse = 1.0 / (jnp.sum(expo, axis=1, keepdims=True) + own_exp)
            weights.append((expo * inverse).astype(BF16))
            own.append((own_exp * inverse).astype(BF16).astype(F32))
        for b, weight, own_weight in zip(members, weights, own):
            mixed = dot_nt(weight, values[b].reshape(lanes, span))
            out_rows[b * 8 : b * 8 + heads, :] = mixed + own_weight * new_values[b : b + 1, :]

    blocks = []
    for h in range(heads):
        kv = h // group
        base = (h * hd) // lanes * lanes
        segment = out_rows[pl.ds(h, rows, stride=8), :]
        segment = jnp.where(lane_kv == kv, segment, 0.0)
        shift = (h * hd - base - kv * hd) % lanes
        if shift:
            segment = pltpu.roll(segment, shift, 1)
        if base // lanes == len(blocks):
            blocks.append(segment)
        else:
            blocks[-1] = blocks[-1] + segment
    wo_copy.wait()
    total = None
    for i, block in enumerate(blocks):
        term = dot(block.astype(BF16), wo[i * lanes : (i + 1) * lanes, :])
        total = term if total is None else total + term
    part[...] = jnp.zeros_like(part)
    part[0:rows, :] = total.astype(BF16)

    sent = []

    def send(src, dst, s_sem, r_sem, target):
        copy = pltpu.make_async_remote_copy(
            src_ref=src,
            dst_ref=dst,
            send_sem=s_sem,
            recv_sem=r_sem,
            device_id=target,
            device_id_type=MESH,
        )
        copy.start()
        sent.append(copy)
        return copy

    pl.semaphore_wait(barrier, len(peers))
    swap = send(part, part_in, t_sem.at[0], t_sem.at[1], device(o, a, c, nt))
    for copy in late_copies:
        copy.wait()
    expert = lax.broadcasted_iota(jnp.int32, (outer, rows), 0)
    row_weights = jnp.zeros((outer, rows), F32)
    for k in range(routes_ref.shape[0]):
        named = routes_ref[k : k + 1, :] == expert
        row_weights = row_weights + jnp.where(named, route_weights_ref[k : k + 1, :], 0.0)
    swap.wait_recv()
    mixed = part[0:rows, :].astype(F32) + part_in[0:rows, :].astype(F32)
    mixed = mixed.astype(BF16).astype(F32)
    summed = (token_f + mixed).astype(BF16).astype(F32)
    for i in range(width // cols):
        residual[i, 0:rows, :] = summed[:, i * cols : (i + 1) * cols]
    ffn_in = (summed * inverse_rms(summed) * ffn_gain_ref[...]).astype(BF16)
    xbuf[c, a, o] = jnp.zeros((pad, width), BF16)
    xbuf[c, a, o, 0:rows, :] = ffn_in

    mine = xbuf.at[c, a, o]
    order = [o] + others
    for i in reversed(range(len(others))):
        send(mine, mine, z_send.at[i], x_recv.at[c, a, o], device(others[i], a, c, t))
    for i, o_ in enumerate(order):
        block, sem = xbuf.at[c, a, o_], x_recv.at[c, a, o_]
        if i:
            pltpu.make_async_copy(block, block, sem).wait()
        send(block, block, a_send.at[i], sem, device(o, na, c, t))
        send(block, block, c_send.at[0, i], sem, device(o, a, nc, t))
    for i, o_ in enumerate(order):
        block, sem = xbuf.at[c, na, o_], x_recv.at[c, na, o_]
        pltpu.make_async_copy(block, block, sem).wait()
        send(block, block, c_send.at[1, i], sem, device(o, a, nc, t))

    def experts(half):
        x = half.reshape(2 * outer * pad, width)
        g = dot(x, gate[...])
        hidden = (g / (1.0 + jnp.exp(-g)) * dot(x, up[...])).astype(BF16)
        return dot(hidden, down[...]).reshape(2, outer, pad, width)

    for a_ in (a, na):
        for o_ in order:
            block, sem = xbuf.at[nc, a_, o_], x_recv.at[nc, a_, o_]
            pltpu.make_async_copy(block, block, sem).wait()
    order = others[::-1] + [o]
    core_out[...] = experts(xbuf[nc]).astype(BF16)
    for o_ in order:
        send(
            core_out.at[:, o_],
            core_in.at[:, o_],
            core_send.at[o_],
            core_recv.at[o_],
            device(o, a, nc, t),
        )
    core_own[...] = experts(xbuf[c])
    targets = ((na, nt), (na, t), (a, nt))
    for o_ in order:
        block = core_in.at[:, o_]
        pltpu.make_async_copy(block, block, core_recv.at[o_]).wait()
        both = core_own[:, o_] + core_in[:, o_].astype(F32)
        for i in range(width // cols):
            plane[:, i, o_] = both[:, :, i * cols : (i + 1) * cols].astype(BF16)
        for i, (a_, t_) in enumerate(targets):
            send(
                plane.at[a_, t_, o_],
                plane_in.at[i, o_],
                plane_send.at[i, o_],
                plane_recv.at[i, o_],
                device(o, a_, c, t_),
            )
    for n, o_ in enumerate(order):
        total = plane[a, t, o_].astype(F32)
        for i in range(len(targets)):
            block = plane_in.at[i, o_]
            pltpu.make_async_copy(block, block, plane_recv.at[i, o_]).wait()
            total = total + plane_in[i, o_].astype(F32)
        if n < len(others):
            back_out[n] = total.astype(BF16)
            send(
                back_out.at[n], back_in.at[o], back_send.at[n], back_recv.at[o], device(o_, a, c, t)
            )
        else:
            back_in[o] = total.astype(BF16)
    for o_ in others:
        block = back_in.at[o_]
        pltpu.make_async_copy(block, block, back_recv.at[o_]).wait()
    result = residual[t, 0:rows, :]
    square = (rows, rows)
    diagonal = lax.broadcasted_iota(jnp.int32, square, 0) == lax.broadcasted_iota(
        jnp.int32, square, 1
    )
    for e in range(outer):
        weight = jnp.sum(
            jnp.where(diagonal, row_weights[e : e + 1, :], 0.0), axis=1, keepdims=True
        )
        result = result + weight * back_in[e, 0:rows, :].astype(F32)
    out_ref[...] = result.astype(BF16)
    for copy in sent:
        copy.wait_send()


def body(
    tokens,
    attn_gain,
    query_weight,
    key_weight,
    value_weight,
    forget_weight,
    forget_bias,
    out_weight,
    key_cache,
    value_cache,
    cum_forget,
    lengths,
    ffn_gain,
    routes,
    route_weights,
    gate_weight,
    up_weight,
    down_weight,
):
    tp_count = lax.axis_size("tp")
    outer = lax.axis_size("ep") // SLICES
    rows, width = tokens.shape
    cols = width // tp_count
    pad = (rows + 15) // 16 * 16
    kv_local, hd = key_cache.shape[1:3]
    lanes = kv_local * hd
    dma = pltpu.SemaphoreType.DMA
    operands = (
        tokens,
        attn_gain.reshape(1, width),
        forget_bias,
        lengths,
        query_weight,
        key_weight,
        value_weight,
        forget_weight.T,
        out_weight,
        key_cache,
        value_cache,
        cum_forget,
        ffn_gain.reshape(1, width),
        routes.T,
        route_weights.T,
        gate_weight,
        up_weight,
        down_weight,
    )
    held = []
    for i, operand in enumerate(operands):
        space = pltpu.SMEM if i in (2, 3) else pltpu.VMEM
        held.append(space(operand.shape[1:] if i >= 15 else operand.shape, operand.dtype))
    return pl.pallas_call(
        functools.partial(layer_kernel, outer),
        out_shape=jax.ShapeDtypeStruct((rows, cols), BF16),
        in_specs=[pl.BlockSpec(memory_space=pltpu.HBM)] * len(operands),
        out_specs=pl.BlockSpec(memory_space=pltpu.VMEM),
        scratch_shapes=held
        + [
            pltpu.VMEM((pad * 8, lanes), F32),
            pltpu.VMEM((pad * 8, lanes), F32),
            pltpu.VMEM((pad * 8, lanes), F32),
            pltpu.VMEM((pad, width), BF16),
            pltpu.VMEM((pad, width), BF16),
            pltpu.VMEM((tp_count, pad, cols), F32),
            pltpu.VMEM((2, 2, outer, pad, width), BF16),
            pltpu.VMEM((2, outer, pad, width), BF16),
            pltpu.VMEM((2, outer, pad, width), BF16),
            pltpu.VMEM((2, outer, pad, width), F32),
            pltpu.VMEM((2, tp_count, outer, pad, cols), BF16),
            pltpu.VMEM((3, outer, pad, cols), BF16),
            pltpu.VMEM((outer - 1, pad, cols), BF16),
            pltpu.VMEM((outer, pad, cols), BF16),
            dma((15,)),
            dma((rows,)),
            dma((rows,)),
            dma((rows,)),
            dma((2,)),
            dma((outer - 1,)),
            dma((outer,)),
            dma((2, outer)),
            dma((2, 2, outer)),
            dma((outer,)),
            dma((outer,)),
            dma((3, outer)),
            dma((3, outer)),
            dma((outer - 1,)),
            dma((outer,)),
        ],
        compiler_params=pltpu.CompilerParams(
            collective_id=0, has_side_effects=True, vmem_limit_bytes=60 * 2**20
        ),
        name="layer",
    )(*operands)


def solution(mesh):
    return jax.shard_map(
        body,
        mesh=mesh,
        in_specs=(
            P("ep", None),
            P(),
            P(None, "tp"),
            P(None, "tp"),
            P(None, "tp"),
            P(None, "tp"),
            P("tp"),
            P("tp", None),
            P("ep", "tp", None, None),
            P("ep", "tp", None, None),
            P("ep", "tp", None),
            P("ep"),
            P(),
            P("ep", None),
            P("ep", None),
            P("ep", None, "tp"),
            P("ep", None, "tp"),
            P("ep", "tp", None),
        ),
        out_specs=P("ep", "tp"),
        check_vma=False,
    )
```

time: 48.7 us -> 31.8 us (0.65)
  local copies, waits for them, and re-layouts: 14.5 us -> 1.32 us
  Pallas kernels: 33.6 us -> 30.2 us
    unnamed x37 -> x1, local copies, waits for them, and re-layouts: 14.5 us -> 1.32 us
    pallas_call x2 -> x1, Pallas kernels: 33.6 us -> 30.2 us  [body(): pl.pallas_call(functools.partial(layer_kernel, outer), out_shape=jax.Shap...]
where the time goes in v2:
time: 31.8 us; the launch traced here: 31.6 us
  Pallas kernels  30.2 us (95%)
  local copies, waits for them, and re-layouts  1.32 us (4%)
    pallas_call x1, Pallas kernels, body(): pl.pallas_call(functools.partial(layer_kernel, outer), out_shape=jax.Shap...  30.2 us
    unnamed x1, local copies, waits for them, and re-layouts  1.32 us

profile of v2, /device:TPU:0, one launch (start us, length us, event | category | flops | bytes accessed | tf_op | source)
XLA Modules:
  0.0 31.6 jit_solution(8741872256574784718)
XLA Ops:
  0.0 30.2 %layer.1 = bf16[13,512]{1,0:T(8,128)(2,1)} custom-call(bf16[13,1024]{1,0:T(8,128)(2,1)} %tokens_hbm.1, f32[1,1024]{1,0:T(1,128)} %bitcast.6, f32[4]{0:T(128)} %bias_hbm.1, s32[13]{0:T(128)} %lengths_hbm.1, bf16[1024,256]{1,0:T(8,128)(2,1)} %wq_hbm.1, bf16[1024,128]{1,0:T(8,128)(2,1)} %wk_hbm.1, bf16[1024,128]{1,0:T(8,128)(2,1)} %wv_hbm.1, ...), custom_call_target="tpu_custom_call" | custom-call | tf_op jit(solution)/shard_map/layer/pallas_call | solution.py:416
  30.2 1.3 %copy.20 = bf16[13,512]{1,0:T(8,128)(2,1)} copy(bf16[13,512]{1,0:T(8,128)(2,1)} %layer.1) | data formatting | bytes 26624

commit v3 on v2

--- a/solution.py
+++ b/solution.py
@@ -13,6 +13,7 @@
 SLICES = 4
 EPSILON = 1e-06
 GROUP_SEQS = 4
+PACK = 2
 MESH = pl.DeviceIdType.MESH
 F32 = jnp.float32
 BF16 = jnp.bfloat16
@@ -191,44 +192,64 @@
         if shift:
             segment = pltpu.roll(segment, shift, 1)
         segment = jnp.where(lane_kv == kv, segment, 0.0)
-        q_rows[pl.ds(h, rows, stride=8), :] = segment
-        own_rows[pl.ds(h, rows, stride=8), :] = segment * new_keys
-
-    position = lax.broadcasted_iota(jnp.int32, (heads, span), 1)
+        q_rows[pl.ds(h, rows, stride=heads), :] = segment
+        own_rows[pl.ds(h, rows, stride=heads), :] = segment * new_keys
+
+    def stacked(pieces):
+        return pieces[0] if len(pieces) == 1 else jnp.concatenate(pieces, axis=0)
+
     for first in range(0, rows, GROUP_SEQS):
-        members = range(first, min(first + GROUP_SEQS, rows))
-        for b in members:
-            for copy in copies[b]:
-                copy.wait()
-        scores = [
-            dot(q_rows[b * 8 : b * 8 + 8, :].astype(BF16), keys[b].reshape(lanes, span))[:heads]
-            for b in members
-        ]
-        weights, own = [], []
-        for b, score in zip(members, scores):
-            cumul = cum[b]
-            length = lengths_ref[b]
+        final = min(first + GROUP_SEQS, rows)
+        packs = [range(b, min(b + PACK, final)) for b in range(first, final, PACK)]
+        scores, weights, own = [], [], []
+        for pack in packs:
+            for b in pack:
+                copies[b][0].wait()
+                copies[b][1].wait()
+            n = len(pack)
+            tile = q_rows[pack[0] * heads : (pack[0] + n) * heads, :]
+            member = lax.broadcasted_iota(jnp.int32, tile.shape, 0) // heads
+            parts = [jnp.where(member == i, tile, 0.0) for i in range(n)]
+            tile = parts[0] if n == 1 else jnp.concatenate(parts, axis=1)
+            block = keys[pack[0] : pack[0] + n].reshape(n * lanes, span)
+            scores.append(dot(tile.astype(BF16), block))
+        for pack, score in zip(packs, scores):
+            n = len(pack)
+            at = slice(pack[0] * heads, (pack[0] + n) * heads)
+            member = lax.broadcasted_iota(jnp.int32, (n * heads, 1), 0) // heads
+            length = jnp.zeros((n * heads, 1), jnp.int32)
+            for i, b in enumerate(pack):
+                length = jnp.where(member == i, lengths_ref[b], length)
+            cumul = stacked([cum[b] for b in pack])
+            forget = stacked([log_forget[:, b : b + 1] for b in pack])
+            position = lax.broadcasted_iota(jnp.int32, (n * heads, span), 1)
             last = jnp.sum(jnp.where(position == length - 1, cumul, 0.0), axis=1, keepdims=True)
-            score = score * scale + (last - cumul) + log_forget[:, b : b + 1]
-            score = jnp.where(position < length, score, -jnp.inf)
-            self_score = (
-                jnp.sum(own_rows[b * 8 : b * 8 + 8, :], axis=1, keepdims=True)[:heads] * scale
-            )
+            score = jnp.where(position < length, score * scale - cumul, -jnp.inf)
+            self_score = jnp.sum(own_rows[at, :], axis=1, keepdims=True) * scale
+            self_score = self_score - (last + forget)
             top = jnp.maximum(jnp.max(score, axis=1, keepdims=True), self_score)
             expo = jnp.exp(score - top)
             own_exp = jnp.exp(self_score - top)
             inverse = 1.0 / (jnp.sum(expo, axis=1, keepdims=True) + own_exp)
             weights.append((expo * inverse).astype(BF16))
             own.append((own_exp * inverse).astype(BF16).astype(F32))
-        for b, weight, own_weight in zip(members, weights, own):
-            mixed = dot_nt(weight, values[b].reshape(lanes, span))
-            out_rows[b * 8 : b * 8 + heads, :] = mixed + own_weight * new_values[b : b + 1, :]
+        for b in range(first, final):
+            copies[b][2].wait()
+        for pack, weight, own_weight in zip(packs, weights, own):
+            n = len(pack)
+            mixed = dot_nt(weight, values[pack[0] : pack[0] + n].reshape(n * lanes, span))
+            member = lax.broadcasted_iota(jnp.int32, (n * heads, lanes), 0) // heads
+            value, fresh = mixed[:, :lanes], new_values[pack[0] : pack[0] + 1, :]
+            for i in range(1, n):
+                value = jnp.where(member == i, mixed[:, i * lanes : (i + 1) * lanes], value)
+                fresh = jnp.where(member == i, new_values[pack[i] : pack[i] + 1, :], fresh)
+            out_rows[pack[0] * heads : (pack[0] + n) * heads, :] = value + own_weight * fresh
 
     blocks = []
     for h in range(heads):
         kv = h // group
         base = (h * hd) // lanes * lanes
-        segment = out_rows[pl.ds(h, rows, stride=8), :]
+        segment = out_rows[pl.ds(h, rows, stride=heads), :]
         segment = jnp.where(lane_kv == kv, segment, 0.0)
         shift = (h * hd - base - kv * hd) % lanes
         if shift:
@@ -387,6 +408,7 @@
     cols = width // tp_count
     pad = (rows + 15) // 16 * 16
     kv_local, hd = key_cache.shape[1:3]
+    heads = cum_forget.shape[1]
     lanes = kv_local * hd
     dma = pltpu.SemaphoreType.DMA
     operands = (
@@ -420,9 +442,9 @@
         out_specs=pl.BlockSpec(memory_space=pltpu.VMEM),
         scratch_shapes=held
         + [
-            pltpu.VMEM((pad * 8, lanes), F32),
-            pltpu.VMEM((pad * 8, lanes), F32),
-            pltpu.VMEM((pad * 8, lanes), F32),
+            pltpu.VMEM((pad * heads, lanes), F32),
+            pltpu.VMEM((pad * heads, lanes), F32),
+            pltpu.VMEM((pad * heads, lanes), F32),
             pltpu.VMEM((pad, width), BF16),
             pltpu.VMEM((pad, width), BF16),
             pltpu.VMEM((tp_count, pad, cols), F32),

time: 31.8 us -> 32.6 us (1.025)
  Pallas kernels: 30.2 us -> 31 us
    pallas_call x1, Pallas kernels: 30.2 us -> 31 us  [body(): pl.pallas_call(functools.partial(layer_kernel, outer), out_shape=jax.Shap...]
where the time goes in v3:
time: 32.6 us; the launch traced here: 32.3 us
  Pallas kernels  31 us (95%)
  local copies, waits for them, and re-layouts  1.32 us (4%)
    pallas_call x1, Pallas kernels, body(): pl.pallas_call(functools.partial(layer_kernel, outer), out_shape=jax.Shap...  31 us
    unnamed x1, local copies, waits for them, and re-layouts  1.32 us

profile of v3, /device:TPU:0, one launch (start us, length us, event | category | flops | bytes accessed | tf_op | source)
XLA Modules:
  0.0 32.3 jit_solution(355202160829272673)
XLA Ops:
  0.0 31.0 %layer.1 = bf16[13,512]{1,0:T(8,128)(2,1)} custom-call(bf16[13,1024]{1,0:T(8,128)(2,1)} %tokens_hbm.1, f32[1,1024]{1,0:T(1,128)} %bitcast.6, f32[4]{0:T(128)} %bias_hbm.1, s32[13]{0:T(128)} %lengths_hbm.1, bf16[1024,256]{1,0:T(8,128)(2,1)} %wq_hbm.1, bf16[1024,128]{1,0:T(8,128)(2,1)} %wk_hbm.1, bf16[1024,128]{1,0:T(8,128)(2,1)} %wv_hbm.1, ...), custom_call_target="tpu_custom_call" | custom-call | tf_op jit(solution)/shard_map/layer/pallas_call | solution.py:438
  31.0 1.3 %copy.20 = bf16[13,512]{1,0:T(8,128)(2,1)} copy(bf16[13,512]{1,0:T(8,128)(2,1)} %layer.1) | data formatting | bytes 26624
